TPU v7x, 32 devices: a whole 2x2x4 slice. The times are simulated.
32 devices in a mesh: rep: 2 (over x), fs: 8 (over z, y), tp: 2 (over core).
Axes of the slice: x: 2, y: 2, z: 4, core: 2. Of those that a mesh axis runs over, the one named last changes fastest.
Arguments:
- tokens: bfloat16 [16, 64, 2048], P(('rep', 'fs'), None, 'tp'), may hold values from -6 to 6
- lin_weight: bfloat16 [2048, 1024], P('fs', 'tp'), may hold values from -0.125 to 0.125
- glu_weight: bfloat16 [2048, 1024], P('fs', 'tp'), may hold values from -0.125 to 0.125
- conv_taps: float32 [31, 1024], P(None, 'tp'), may hold values from -4 to 4
- conv_gain: float32 [1024], P('tp'), may hold values from 0.1 to 1.9
- conv_out_weight: bfloat16 [1024, 2048], P('tp', 'fs'), may hold values from -0.1875 to 0.1875
- mix_gain: float32 [2048], replicated, may hold values from 0.1 to 1.9
- ff_gate: bfloat16 [2048, 5632], P('fs', 'tp'), may hold values from -0.125 to 0.125
- ff_up: bfloat16 [2048, 5632], P('fs', 'tp'), may hold values from -0.125 to 0.125
- ff_down: bfloat16 [5632, 2048], P('tp', 'fs'), may hold values from -0.078125 to 0.078125
- out_gain: float32 [2048], replicated, may hold values from 0.1 to 1.9
Outputs:
- encoded: bfloat16 [16, 64, 2048], P(('rep', 'fs'), None, 'tp')
All inputs are finite; a program needn't handle non-finite values.
Results may differ from a plain program's by a relative error of at most 0.014.
Values may be sent and summed in bfloat16 or wider, within the bound.
A program may use at most 128 MiB of HBM per device.

v0:
```python
import jax
import jax.numpy as jnp
from jax import lax
from jax.sharding import PartitionSpec as P

D = 2048
CONV = 1024
TAPS = 31


residual_scale = 2.0**0.25
epsilon = 1e-05


def rounded(value):
    return lax.optimization_barrier(value.astype(jnp.bfloat16)).astype(jnp.float32)


def scaled(values, totals, squares, count):
    average = totals[:, None] / count
    second = squares[:, None] / count
    return (values - average) * lax.rsqrt(second - average * average + epsilon)


def on_device(
    tokens,
    lin_weight,
    glu_weight,
    conv_taps,
    conv_gain,
    conv_out_weight,
    mix_gain,
    ff_gate,
    ff_up,
    ff_down,
    out_gain,
):
    own_tokens = tokens[0]
    feat_width = own_tokens.shape[1]
    offset = lax.axis_index("tp") * feat_width
    all_tokens = lax.all_gather(own_tokens, "tp", axis=1, tiled=True)
    seq_rows = all_tokens.shape[0]
    pieces = (
        lax.all_gather(lin_weight, "fs", axis=0, tiled=True),
        lax.all_gather(glu_weight, "fs", axis=0, tiled=True),
    )
    columns = all_tokens
    linear = jnp.dot(columns, pieces[0], preferred_element_type=jnp.float32)
    gating = jnp.dot(columns, pieces[1], preferred_element_type=jnp.float32)
    glu = (linear * jax.nn.sigmoid(gating)).astype(jnp.bfloat16)
    margin = (TAPS - 1) // 2
    conv = lax.conv_general_dilated(
        glu.astype(jnp.float32)[None],
        conv_taps[:, None, :],
        (1,),
        [(margin, margin)],
        dimension_numbers=("NWC", "WIO", "NWC"),
        feature_group_count=glu.shape[1],
        precision=lax.Precision.HIGHEST,
    )[0]
    conv_sums, conv_squares = lax.psum((jnp.sum(conv, axis=1), jnp.sum(conv * conv, axis=1)), "tp")
    activated = jax.nn.silu(scaled(conv, conv_sums, conv_squares, CONV) * conv_gain).astype(
        jnp.bfloat16
    )
    conv_terms = jnp.dot(
        activated,
        lax.all_gather(conv_out_weight, "fs", axis=1, tiled=True),
        preferred_element_type=jnp.float32,
    )
    mixed = rounded(
        lax.psum_scatter(
            conv_terms.astype(jnp.bfloat16), "tp", scatter_dimension=1, tiled=True
        ).astype(jnp.float32)
    )
    before = residual_scale * own_tokens.astype(jnp.float32) + mixed
    mix_sums, mix_squares = lax.psum(
        (jnp.sum(before, axis=1), jnp.sum(before * before, axis=1)), "tp"
    )
    gain_own = lax.dynamic_slice_in_dim(mix_gain, offset, feat_width, 0)
    middle_own = (scaled(before, mix_sums, mix_squares, D) * gain_own).astype(jnp.bfloat16)
    middle_all = lax.all_gather(middle_own, "tp", axis=1, tiled=True)
    empty_ffn = jnp.zeros((seq_rows, ff_gate.shape[1]), jnp.float32)
    pieces = (
        lax.all_gather(ff_gate, "fs", axis=0, tiled=True),
        lax.all_gather(ff_up, "fs", axis=0, tiled=True),
    )
    columns = lax.slice_in_dim(middle_all, 0, pieces[0].shape[0], axis=1)
    gate = empty_ffn + jnp.dot(columns, pieces[0], preferred_element_type=jnp.float32)
    upward = empty_ffn + jnp.dot(columns, pieces[1], preferred_element_type=jnp.float32)
    hidden = (jax.nn.silu(gate) * upward).astype(jnp.bfloat16)
    down_terms = jnp.dot(
        hidden,
        lax.all_gather(ff_down, "fs", axis=1, tiled=True),
        preferred_element_type=jnp.float32,
    )
    forward = rounded(
        lax.psum_scatter(
            down_terms.astype(jnp.bfloat16), "tp", scatter_dimension=1, tiled=True
        ).astype(jnp.float32)
    )
    final = residual_scale * middle_own.astype(jnp.float32) + forward
    out_sums, out_squares = lax.psum((jnp.sum(final, axis=1), jnp.sum(final * final, axis=1)), "tp")
    gain_slice = lax.dynamic_slice_in_dim(out_gain, offset, feat_width, 0)
    encoded = (scaled(final, out_sums, out_squares, D) * gain_slice).astype(jnp.bfloat16)
    return encoded[None]


def solution(mesh):
    return jax.shard_map(
        on_device,
        mesh=mesh,
        in_specs=(
            P(("rep", "fs"), None, "tp"),
            P("fs", "tp"),
            P("fs", "tp"),
            P(None, "tp"),
            P("tp"),
            P("tp", "fs"),
            P(),
            P("fs", "tp"),
            P("fs", "tp"),
            P("tp", "fs"),
            P(),
        ),
        out_specs=P(("rep", "fs"), None, "tp"),
        check_vma=False,
    )
```

profile of v0, /device:TPU:11, one launch (start us, length us, event | category | flops | bytes accessed | tf_op | source)
XLA Modules:
  0.0 694.3 jit_solution(6831628930254306742)
XLA Ops:
  6.5 0.7 all-gather.8.cloned.1.call-update
  7.3 0.7 all-gather.10.cloned.1.call-update
  8.1 0.7 all-gather.12.cloned.1.call-update
  8.7 0.0 reduce-scatter.3.cloned.1.call-start
  8.8 2.5 all-gather
  11.3 47.4 %all-gather.8.cloned.1.call-done = bf16[2048,512]{1,0:T(8,128)(2,1)} async-done(((bf16[256,512]{1,0:T(8,128)(2,1)}), bf16[2048,512]{1,0:T(8,128)(2,1)}) %all-gather.8.cloned.1.call-update) | async-done | bytes 2097168 | tf_op jit(solution)/shard_map/all_gather | solution.py:44
  58.7 2.1 fusion.9
  60.8 47.7 %all-gather.10.cloned.1.call-done = bf16[2048,512]{1,0:T(8,128)(2,1)} async-done(((bf16[256,512]{1,0:T(8,128)(2,1)}), bf16[2048,512]{1,0:T(8,128)(2,1)}) %all-gather.10.cloned.1.call-update) | async-done | bytes 2097168 | tf_op jit(solution)/shard_map/all_gather | solution.py:45
  108.5 2.1 fusion.6
  110.6 1.3 fusion.26
  111.9 0.1 fusion.16
  112.0 3.9 all-reduce.2
  115.9 42.1 %all-gather.12.cloned.1.call-done = bf16[512,2048]{1,0:T(8,128)(2,1)} async-done(((bf16[512,256]{1,0:T(8,128)(2,1)}), bf16[512,2048]{1,0:T(8,128)(2,1)}) %all-gather.12.cloned.1.call-update) | async-done | bytes 2097168 | tf_op jit(solution)/shard_map/all_gather | solution.py:67
  158.0 2.8 convolution_convert_fusion.1
  160.9 0.0 all-gather.14.cloned.1.call-start
  160.9 0.5 all-gather.14.cloned.1.call-update
  161.5 0.5 all-gather.16.cloned.1.call-update
  162.1 0.7 all-gather.18.cloned.1.call-update
  162.9 7.2 %reduce-scatter.3.cloned.1.call-done = bf16[64,1024]{1,0:T(8,128)(2,1)} async-done(((bf16[64,2048]{1,0:T(8,128)(2,1)}), bf16[64,1024]{1,0:T(8,128)(2,1)}) %reduce-scatter.3.cloned.1.call-update) | async-done | bytes 131088 | tf_op jit(solution)/shard_map/reduce_scatter | solution.py:71
  170.1 1.1 fusion.12
  171.2 2.5 all-reduce.1
  173.7 1.0 multiply_convert_fusion.1
  174.7 2.0 all_gather.28
  176.7 156.6 %all-gather.14.cloned.1.call-done = bf16[2048,2816]{1,0:T(8,128)(2,1)} async-done(((bf16[256,2816]{1,0:T(8,128)(2,1)}), bf16[2048,2816]{1,0:T(8,128)(2,1)}) %all-gather.14.cloned.1.call-update) | async-done | bytes 11534352 | tf_op jit(solution)/shard_map/all_gather | solution.py:84
  333.3 6.4 fusion.27
  339.7 157.2 %all-gather.16.cloned.1.call-done = bf16[2048,2816]{1,0:T(8,128)(2,1)} async-done(((bf16[256,2816]{1,0:T(8,128)(2,1)}), bf16[2048,2816]{1,0:T(8,128)(2,1)}) %all-gather.16.cloned.1.call-update) | async-done | bytes 11534352 | tf_op jit(solution)/shard_map/all_gather | solution.py:85
  496.9 163.6 %all-gather.18.cloned.1.call-done = bf16[2816,2048]{1,0:T(8,128)(2,1)} async-done(((bf16[2816,256]{1,0:T(8,128)(2,1)}), bf16[2816,2048]{1,0:T(8,128)(2,1)}) %all-gather.18.cloned.1.call-update) | async-done | bytes 11534352 | tf_op jit(solution)/shard_map/all_gather | solution.py:93
  660.5 12.4 %convolution_convert_fusion = bf16[64,2048]{1,0:T(8,128)(2,1)} fusion(bf16[2816,2048]{1,0:T(8,128)(2,1)} %all-gather.18.cloned.1.call-done, bf16[64,2048]{1,0:T(8,128)(2,1)S(1)} %all_gather.28, bf16[2048,2816]{1,0:T(8,128)(2,1)} %all-gather.16.cloned.1.call-done, f32[64,2816]{1,0:T(8,128)S(1)} %fusion.27), kind=kOutput, calls=%fused_computation.2 | convolution fusion | flops 1477607424 | bytes 24313856 | tf_op jit(solution)/shard_map/dot_general | solution.py:91
  672.9 9.4 %reduce-scatter.5.cloned.1.call-done = bf16[64,1024]{1,0:T(8,128)(2,1)} async-done(((bf16[64,2048]{1,0:T(8,128)(2,1)}), bf16[64,1024]{1,0:T(8,128)(2,1)}) %reduce-scatter.5.cloned.1.call-update) | async-done | bytes 131088 | tf_op jit(solution)/shard_map/reduce_scatter | solution.py:97
  682.2 1.1 fusion.11
  683.3 2.5 all-reduce
  685.8 1.7 fusion.13
  (22 shorter events, 0.3 us)
Async XLA Ops:
  6.5 104.0 %copy-start = (f32[31,512]{1,0:T(8,128)S(1)}, f32[31,512]{1,0:T(8,128)}, u32[]{:S(2)}) copy-start(f32[31,512]{1,0:T(8,128)} %param.14) | copy-start | bytes 190468
  6.5 52.1 %all-gather.8.cloned.1.call-start = ((), (), s32[]{:S(2)}) async-start(), calls=%async_computation.2 | async-start | bytes 2359296 | tf_op jit(solution)/shard_map/all_gather | solution.py:44
  7.3 101.2 %all-gather.10.cloned.1.call-start = ((), (), s32[]{:S(2)}) async-start(), calls=%async_computation.3 | async-start | bytes 2359296 | tf_op jit(solution)/shard_map/all_gather | solution.py:45
  8.0 150.0 %all-gather.12.cloned.1.call-start = ((), (), s32[]{:S(2)}) async-start(), calls=%async_computation.4 | async-start | bytes 2359296 | tf_op jit(solution)/shard_map/all_gather | solution.py:67
  8.7 161.4 %reduce-scatter.3.cloned.1.call-start = ((), (), s32[]{:S(2)}) async-start(), calls=%async_computation.5 | async-start | bytes 393216 | tf_op jit(solution)/shard_map/reduce_scatter | solution.py:71
  60.8 97.2 %copy-start.3 = (f32[512]{0:T(512)S(1)}, f32[512]{0:T(512)}, u32[]{:S(2)}) copy-start(f32[512]{0:T(512)} %param.15) | copy-start | bytes 6148
  160.9 2.0 copy-start.2
  160.9 9.3 %copy-start.1 = (bf16[1,64,1024]{2,1,0:T(8,128)(2,1)S(1)}, bf16[1,64,1024]{2,1,0:T(8,128)(2,1)}, u32[]{:S(2)}) copy-start(bf16[1,64,1024]{2,1,0:T(8,128)(2,1)} %param.11) | copy-start | bytes 393220
  160.9 172.5 %all-gather.14.cloned.1.call-start = ((), (), s32[]{:S(2)}) async-start(), calls=%async_computation.6 | async-start | bytes 12976128 | tf_op jit(solution)/shard_map/all_gather | solution.py:84
  161.5 335.4 %all-gather.16.cloned.1.call-start = ((), (), s32[]{:S(2)}) async-start(), calls=%async_computation.7 | async-start | bytes 12976128 | tf_op jit(solution)/shard_map/all_gather | solution.py:85
  162.0 498.4 %all-gather.18.cloned.1.call-start = ((), (), s32[]{:S(2)}) async-start(), calls=%async_computation.8 | async-start | bytes 12976128 | tf_op jit(solution)/shard_map/all_gather | solution.py:93
  162.8 519.4 %reduce-scatter.5.cloned.1.call-start = ((), (), s32[]{:S(2)}) async-start(), calls=%async_computation.9 | async-start | bytes 393216 | tf_op jit(solution)/shard_map/reduce_scatter | solution.py:97
  339.7 346.1 %dynamic-slice-start = ((f32[2048]{0:T(1024)}, s32[]{:T(128)}), f32[1024]{0:T(1024)S(1)}, s32[]{:S(2)}) async-start(f32[2048]{0:T(1024)} %param.21, s32[]{:T(128)} %select_n.4), calls=%async_computation.10 | async-start | bytes 8704 | tf_op jit(solution)/shard_map/dynamic_slice | solution.py:103
Sparse Core Ops, SparseCore 0:
  9.5 49.1 all-gather.7
  60.8 47.6 all-gather.9
  110.5 47.4 all-gather.11
  161.0 9.1 reduce-scatter.2
  172.2 161.1 all-gather.13
  335.4 161.4 all-gather.15
  498.9 161.4 all-gather.17
  673.0 9.2 reduce-scatter.4
where the time goes:
time: 696 us; the launch traced here: 694 us
  waiting for transfers between devices  635 us (91%)
  matrix products  27 us (4%)
  between operations  13.6 us (2%)
  blocking collectives  13.3 us (2%)
    all_gather x1, waiting for transfers between devices, on_device(): lax.all_gather(ff_down, 'fs', axis=1, tiled=True)  164 us
    all_gather x1, waiting for transfers between devices, on_device(): lax.all_gather(ff_up, 'fs', axis=0, tiled=True)  157 us
    all_gather x1, waiting for transfers between devices, on_device(): lax.all_gather(ff_gate, 'fs', axis=0, tiled=True)  157 us
    all_gather x1, waiting for transfers between devices, on_device(): lax.all_gather(glu_weight, 'fs', axis=0, tiled=True)  47.7 us
    all_gather x1, waiting for transfers between devices, on_device(): lax.all_gather(lin_weight, 'fs', axis=0, tiled=True)  47.4 us
    all_gather x1, waiting for transfers between devices, on_device(): lax.all_gather(conv_out_weight, 'fs', axis=1, tiled=True)  42.1 us
  transfers between devices with their start and end apart: 8, of which 8 were waited for; matrix products, arithmetic and copies ran while one was open for 2% of the time, Pallas kernels for 0%

commit v1 on v0

v1 whole, which is shorter than its diff:
```python
import jax
import jax.numpy as jnp
from jax import lax
from jax.sharding import PartitionSpec as P

residual_scale = 2.0**0.25
epsilon = 1e-05


def normed(values):
    average = jnp.mean(values, axis=-1, keepdims=True)
    second = jnp.mean(values * values, axis=-1, keepdims=True)
    return (values - average) * lax.rsqrt(second - average * average + epsilon)


def interleave(left, right, parts):
    rows, width = left.shape
    pair = jnp.concatenate(
        (left.reshape(rows, parts, width // parts), right.reshape(rows, parts, width // parts)),
        axis=2,
    )
    return pair.reshape(rows, 2 * width)


def on_device(
    tokens,
    lin_weight,
    glu_weight,
    conv_taps,
    conv_gain_all,
    conv_out_weight,
    mix_gain,
    ff_gate,
    ff_up,
    ff_down,
    out_gain,
):
    n_fs, n_tp = lax.axis_size("fs"), lax.axis_size("tp")
    fs_index, tp_index = lax.axis_index("fs"), lax.axis_index("tp")
    seqs, length, feat = tokens.shape
    groups = n_fs * seqs
    rows = groups * length
    model = feat * n_tp

    gathered = lax.all_gather(tokens, ("fs", "tp"), axis=0, tiled=False)
    all_tokens = (
        gathered.reshape(n_fs, n_tp, seqs, length, feat)
        .transpose(0, 2, 3, 1, 4)
        .reshape(rows, model)
    )
    glu_pair = lax.all_to_all(
        interleave(lin_weight, glu_weight, n_fs), "fs", split_axis=1, concat_axis=0, tiled=True
    )
    own_out = lax.all_to_all(conv_out_weight, "tp", split_axis=1, concat_axis=0, tiled=True)
    ff_pair = lax.all_to_all(
        interleave(ff_gate, ff_up, n_fs), "fs", split_axis=1, concat_axis=0, tiled=True
    )
    own_down = lax.all_to_all(ff_down, "fs", split_axis=0, concat_axis=1, tiled=True)

    chans = glu_pair.shape[1] // 2
    product = jnp.dot(all_tokens, glu_pair, preferred_element_type=jnp.float32)
    glu = (product[:, :chans] * jax.nn.sigmoid(product[:, chans:])).astype(jnp.bfloat16)
    n_taps = conv_taps.shape[0]
    margin = (n_taps - 1) // 2
    own_taps = lax.dynamic_slice_in_dim(conv_taps, fs_index * chans, chans, 1)
    padded = jnp.pad(
        glu.astype(jnp.float32).reshape(groups, length, chans),
        ((0, 0), (margin, margin), (0, 0)),
    )
    conv = sum(padded[:, k : k + length] * own_taps[k] for k in range(n_taps))
    conv = conv.reshape(rows, chans).astype(jnp.bfloat16)
    conv_all = lax.all_gather(conv, ("tp", "fs"), axis=1, tiled=True)
    activated = jax.nn.silu(normed(conv_all.astype(jnp.float32)) * conv_gain_all).astype(
        jnp.bfloat16
    )
    mixed_own = jnp.dot(activated, own_out, preferred_element_type=jnp.float32).astype(
        jnp.bfloat16
    )
    mixed = lax.all_gather(mixed_own, ("fs", "tp"), axis=1, tiled=True)
    before = residual_scale * all_tokens.astype(jnp.float32) + mixed.astype(jnp.float32)
    middle = (normed(before) * mix_gain).astype(jnp.bfloat16)

    units = ff_pair.shape[1] // 2
    both = jnp.dot(middle, ff_pair, preferred_element_type=jnp.float32)
    hidden = (jax.nn.silu(both[:, :units]) * both[:, units:]).astype(jnp.bfloat16)
    down = jnp.dot(hidden, own_down, preferred_element_type=jnp.float32).astype(jnp.bfloat16)
    sends = (
        down.reshape(n_fs, seqs * length, n_tp, feat)
        .transpose(0, 2, 1, 3)
        .reshape(n_fs * n_tp, seqs * length, feat)
    )
    arrived = lax.all_to_all(sends, ("fs", "tp"), split_axis=0, concat_axis=0, tiled=True)
    forward = jnp.sum(arrived.astype(jnp.float32), axis=0)
    forward = forward.astype(jnp.bfloat16).astype(jnp.float32)
    middle_own = lax.dynamic_slice(
        middle,
        (fs_index * seqs * length, tp_index * feat),
        (seqs * length, feat),
    )
    final = residual_scale * middle_own.astype(jnp.float32) + forward
    sums, squares = lax.psum(
        (jnp.sum(final, axis=1, keepdims=True), jnp.sum(final * final, axis=1, keepdims=True)),
        "tp",
    )
    average = sums / model
    out = (final - average) * lax.rsqrt(squares / model - average * average + epsilon)
    gain = lax.dynamic_slice_in_dim(out_gain, tp_index * feat, feat, 0)
    return (out * gain).astype(jnp.bfloat16).reshape(seqs, length, feat)


def solution(mesh):
    mapped = jax.shard_map(
        on_device,
        mesh=mesh,
        in_specs=(
            P(("rep", "fs"), None, "tp"),
            P("fs", "tp"),
            P("fs", "tp"),
            P(None, "tp"),
            P(),
            P("tp", "fs"),
            P(),
            P("fs", "tp"),
            P("fs", "tp"),
            P("tp", "fs"),
            P(),
        ),
        out_specs=P(("rep", "fs"), None, "tp"),
        check_vma=False,
    )
    return mapped
```

time: 696 us -> 279 us (0.40)
  waiting for transfers between devices: 635 us -> 161 us
  local copies, waits for them, and re-layouts: 0.04 us -> 34 us
  starting transfers between devices: 0.27 us -> 27.8 us
  other arithmetic: 4.95 us -> 25.8 us
  matrix products: 27 us -> 9.17 us
  blocking collectives: 13.3 us -> 5.76 us
    all_gather x6 -> x3, waiting for transfers between devices: 615 us -> 57.3 us  [the longest x1 21.4 us: on_device(): mixed = lax.all_gather(mixed_own, ('fs', 'tp'), axis=1, tiled=True)]
    all_to_all x0 -> x5, waiting for transfers between devices: none -> 103 us  [the longest x1 46.1 us: on_device(): lax.all_to_all(sends, ('fs', 'tp'), split_axis=0, concat_axis=0, tiled=True)]
    all_to_all x0 -> x5, starting transfers between devices: none -> 27.8 us  [the longest x1 6.9 us: on_device(): lax.all_to_all(conv_out_weight, 'tp', split_axis=1, concat_axis=0, tiled=...]
    reduce_scatter x2 -> x0, waiting for transfers between devices: 16.6 us -> none  [the longest x1 9.38 us: on_device(): lax.psum_scatter(down_terms.astype(jnp.bfloat16), 'tp', scatter_dimension...]
    dot_general x5 -> x4, matrix products: 25.7 us -> 9.17 us  [the longest x1 2.93 us: on_device(): jnp.dot(activated, own_out, preferred_element_type=jnp.float32)]
    convert_element_type x1 -> x2, other arithmetic: 1.01 us -> 13.1 us  [the longest x1 12.1 us: on_device(): conv = conv.reshape(rows, chans).astype(jnp.bfloat16)]
    reshape x0 -> x4, local copies, waits for them, and re-layouts: none -> 10.7 us  [the longest x2 5.28 us: on_device(): down.reshape(n_fs, seqs * length, n_tp, feat).transpose(0, 2, 1, 3)]
    unnamed x8 -> x22, local copies, waits for them, and re-layouts: 0.02 us -> 10.2 us
  transfers between devices with their start and end apart: 8 -> 8, of which waited for: 8 -> 7; matrix products, arithmetic and copies ran while one was open for 2% -> 18% of each run, Pallas kernels for 0% -> 0%
where the time goes in v1:
time: 279 us; the launch traced here: 277 us
  waiting for transfers between devices  161 us (58%)
  local copies, waits for them, and re-layouts  34 us (12%)
  starting transfers between devices  27.8 us (10%)
  other arithmetic  25.8 us (9%)
  between operations  13.3 us (5%)
  matrix products  9.17 us (3%)
  blocking collectives  5.76 us (2%)
    all_to_all x1, waiting for transfers between devices, on_device(): lax.all_to_all(sends, ('fs', 'tp'), split_axis=0, concat_axis=0, tiled=True)  46.1 us
    all_to_all x1, waiting for transfers between devices, on_device(): lax.all_to_all(interleave(ff_gate, ff_up, n_fs), 'fs', split_axis=1, conc...  39 us
    all_gather x1, waiting for transfers between devices, on_device(): mixed = lax.all_gather(mixed_own, ('fs', 'tp'), axis=1, tiled=True)  21.4 us
    all_gather x1, waiting for transfers between devices, on_device(): conv_all = lax.all_gather(conv, ('tp', 'fs'), axis=1, tiled=True)  20.7 us
    all_gather x1, waiting for transfers between devices, on_device(): gathered = lax.all_gather(tokens, ('fs', 'tp'), axis=0, tiled=False)  15.3 us
    convert_element_type x1, other arithmetic, on_device(): conv = conv.reshape(rows, chans).astype(jnp.bfloat16)  12.1 us
    all_to_all x1, waiting for transfers between devices, on_device(): lax.all_to_all(interleave(lin_weight, glu_weight, n_fs), 'fs', split_axis...  10.9 us
    unnamed x22, local copies, waits for them, and re-layouts  10.2 us
  transfers between devices with their start and end apart: 8, of which 7 were waited for; matrix products, arithmetic and copies ran while one was open for 18% of the time, Pallas kernels for 0%

profile of v1, /device:TPU:11, one launch (start us, length us, event | category | flops | bytes accessed | tf_op | source)
XLA Modules:
  0.0 276.8 jit_solution(18404688022100981771)
XLA Ops:
  10.3 5.7 %all-to-all-start = ((bf16[256,8,128]{0,2,1:T(8,128)(2,1)}), bf16[256,8,128]{0,2,1:T(8,128)(2,1)S(1)}, u32[]{:S(2)}, u32[]{:S(2)}) async-start(bf16[256,8,128]{0,2,1:T(8,128)(2,1)} %pad_maximum_fusion.1), calls=%async_computation | async-start | bytes 1048576 | tf_op jit(solution)/shard_map/all_to_all | solution.py:51
  18.5 1.8 dynamic-slice_bitcast_fusion.30
  20.3 10.9 %all-to-all-done = bf16[256,8,128]{0,2,1:T(8,128)(2,1)S(1)} async-done(((bf16[256,8,128]{0,2,1:T(8,128)(2,1)}), bf16[256,8,128]{0,2,1:T(8,128)(2,1)S(1)}, u32[]{:S(2)}, u32[]{:S(2)}) %all-to-all-start) | async-done | bytes 524320 | tf_op jit(solution)/shard_map/all_to_all | solution.py:51
  31.2 6.9 %all-to-all-start.1 = ((bf16[512,2,128]{0,2,1:T(8,128)(2,1)}), bf16[512,2,128]{0,2,1:T(8,128)(2,1)S(1)}, u32[]{:S(2)}, u32[]{:S(2)}) async-start(bf16[512,2,128]{0,2,1:T(8,128)(2,1)} %bitcast.40), calls=%async_computation.1 | async-start | bytes 524288 | tf_op jit(solution)/shard_map/all_to_all | solution.py:54
  39.1 15.3 %all-gather.11.cloned.1.call-done = bf16[16,64,1024]{2,1,0:T(8,128)(2,1)} async-done(((bf16[1,64,1024]{2,1,0:T(8,128)(2,1)}), bf16[16,64,1024]{2,1,0:T(8,128)(2,1)}) %all-gather.11.cloned.1.call-update) | async-done | bytes 2097168 | tf_op jit(solution)/shard_map/all_gather | solution.py:45
  54.4 3.7 %copy.33 = bf16[8,2,1,64,1024]{4,1,3,0,2:T(2,128)(2,1)S(1)} copy(bf16[8,2,1,64,1024]{4,3,1,0,2:T(8,128)(2,1)} %bitcast.118) | data formatting | bytes 4194304 | tf_op jit(solution)/shard_map/reshape | solution.py:47
  59.5 4.9 %all-to-all-start.3 = ((bf16[8,352,256]{2,1,0:T(8,128)(2,1)}), bf16[8,352,256]{2,1,0:T(8,128)(2,1)S(1)}, u32[]{:S(2)}, u32[]{:S(2)}) async-start(bf16[8,352,256]{2,1,0:T(8,128)(2,1)} %bitcast.121), calls=%async_computation.3 | async-start | bytes 2883584 | tf_op jit(solution)/shard_map/all_to_all | solution.py:58
  64.4 1.9 convolution_bitcast_fusion
  66.9 1.7 reshape.133
  68.6 12.1 %add_convert_fusion = bf16[8,64,64]{1,0,2:T(8,128)(2,1)} fusion(f32[8,64,64]{1,0,2:T(8,128)} %reshape.133, f32[64]{0:T(128)} %get-tuple-element.43, f32[64]{0:T(128)S(1)} %get-tuple-element.14, f32[64]{0:T(128)S(1)} %get-tuple-element.15, f32[64]{0:T(128)S(1)} %get-tuple-element.16, f32[64]{0:T(128)} %get-tuple-element.17, f32[64]{0:T(128)} %get-tuple-element.18, ...), kind=kLoop, calls=%fused_computation.27 | loop fusion | flops 2031616 | bytes 204544 | tf_op jit(solution)/shard_map/convert_element_type | solution.py:71
  80.7 1.7 convert_element_type.50
  82.4 2.6 copy.39
  85.0 2.5 copy.40
  87.6 3.6 %pad_maximum_fusion = bf16[256,8,704]{0,2,1:T(8,128)(2,1)} fusion(bf16[256,8,352]{0,2,1:T(8,128)(2,1)} %bitcast.116, bf16[256,8,352]{0,2,1:T(8,128)(2,1)} %bitcast.115), kind=kLoop, calls=%fused_computation.8 | loop fusion | flops 5767168 | bytes 5767168 | tf_op jit(solution)/shard_map/concatenate | solution.py:18
  91.1 6.9 %all-to-all-done.3 = bf16[8,352,256]{2,1,0:T(8,128)(2,1)S(1)} async-done(((bf16[8,352,256]{2,1,0:T(8,128)(2,1)}), bf16[8,352,256]{2,1,0:T(8,128)(2,1)S(1)}, u32[]{:S(2)}, u32[]{:S(2)}) %all-to-all-start.3) | async-done | bytes 1441824 | tf_op jit(solution)/shard_map/all_to_all | solution.py:58
  98.0 5.9 %all-to-all-start.2 = ((bf16[256,8,704]{0,2,1:T(8,128)(2,1)}), bf16[256,8,704]{0,2,1:T(8,128)(2,1)}, u32[]{:S(2)}, u32[]{:S(2)}) async-start(bf16[256,8,704]{0,2,1:T(8,128)(2,1)} %pad_maximum_fusion), calls=%async_computation.2 | async-start | bytes 5767168 | tf_op jit(solution)/shard_map/all_to_all | solution.py:55
  103.9 1.8 copy.38
  105.7 3.3 %all-gather.2 = f32[2,1,512]{2,1,0:T(1,128)S(1)} all-gather(f32[1,1,512]{2,1,0:T(1,128)S(1)} %bitcast.128), channel_id=3, replica_groups=mesh['rep'=2,'fs'=8,'tp'=2] {'tp'}, dimensions={0}, use_global_device_ids=true | all-gather | bytes 6144 | tf_op args[4]
  109.0 20.7 %all-gather.7.cloned.1.call-done = bf16[512,1024]{0,1:T(8,128)(2,1)} async-done(((bf16[512,64]{0,1:T(8,128)(2,1)}), bf16[512,1024]{0,1:T(8,128)(2,1)}) %all-gather.7.cloned.1.call-update) | async-done | bytes 1048592 | tf_op jit(solution)/shard_map/all_gather | solution.py:72
  131.2 2.9 %convolution_convert_fusion.1 = bf16[512,128]{1,0:T(8,128)(2,1)} fusion(bf16[1024,128]{1,0:T(8,128)(2,1)} %bitcast.126, bf16[512,1024]{0,1:T(8,128)(2,1)} %all-gather.7.cloned.1.call-done, f32[1024]{0:T(1024)S(1)} %bitcast.127, f32[512]{0:T(512)S(1)} %get-tuple-element.47, f32[512]{0:T(512)S(1)} %get-tuple-element.46), kind=kOutput, calls=%fused_computation.19 | convolution fusion | flops 139001856 | bytes 1449984 | tf_op jit(solution)/shard_map/dot_general | solution.py:76
  135.6 39.0 %all-to-all-done.2 = bf16[256,8,704]{0,2,1:T(8,128)(2,1)} async-done(((bf16[256,8,704]{0,2,1:T(8,128)(2,1)}), bf16[256,8,704]{0,2,1:T(8,128)(2,1)}, u32[]{:S(2)}, u32[]{:S(2)}) %all-to-all-start.2) | async-done | bytes 2883616 | tf_op jit(solution)/shard_map/all_to_all | solution.py:55
  174.6 3.8 %copy.44 = bf16[8,88,8,256]{3,2,0,1:T(8,128)(2,1)} copy(bf16[8,88,8,256]{3,2,1,0:T(8,128)(2,1)} %bitcast.56) | data formatting | bytes 5767168 | tf_op jit(solution)/shard_map/all_to_all | solution.py:55
  178.4 21.4 %all-gather.9.cloned.1.call-done = bf16[512,2048]{1,0:T(8,128)(2,1)} async-done(((bf16[512,128]{1,0:T(8,128)(2,1)}), bf16[512,2048]{1,0:T(8,128)(2,1)}) %all-gather.9.cloned.1.call-update) | async-done | bytes 2097168 | tf_op jit(solution)/shard_map/all_gather | solution.py:79
  199.8 2.8 %fusion = (f32[512]{0:T(512)S(1)}, f32[512]{0:T(512)S(1)}) fusion(bf16[512,2048]{1,0:T(8,128)(2,1)} %all-gather.9.cloned.1.call-done, bf16[512,2048]{1,0:T(8,128)(2,1)S(1)} %bitcast.110), kind=kLoop, calls=%fused_computation.3 | loop fusion | flops 7339008 | bytes 4198400 | tf_op jit(solution)/shard_map/reduce_sum | solution.py:11
  204.4 1.7 fusion.39
  206.1 2.7 convolution_convert_fusion
  208.8 3.3 %reshape.129 = bf16[8,64,2,1024]{3,2,1,0:T(2,128)(2,1)S(1)} reshape(bf16[512,2048]{1,0:T(8,128)(2,1)} %convolution_convert_fusion) | data formatting | bytes 4194304 | tf_op jit(solution)/shard_map/reshape | solution.py:88
  212.1 2.0 copy.43
  214.1 4.4 %all-to-all-start.4 = ((bf16[16,64,1024]{2,1,0:T(8,128)(2,1)}), bf16[16,64,1024]{2,1,0:T(8,128)(2,1)S(1)}, u32[]{:S(2)}, u32[]{:S(2)}) async-start(bf16[16,64,1024]{2,1,0:T(8,128)(2,1)} %bitcast.112), calls=%async_computation.4 | async-start | bytes 4194304 | tf_op jit(solution)/shard_map/all_to_all | solution.py:92
  218.5 46.1 %all-to-all-done.4 = bf16[16,64,1024]{2,1,0:T(8,128)(2,1)S(1)} async-done(((bf16[16,64,1024]{2,1,0:T(8,128)(2,1)}), bf16[16,64,1024]{2,1,0:T(8,128)(2,1)S(1)}, u32[]{:S(2)}, u32[]{:S(2)}) %all-to-all-start.4) | async-done | bytes 2097184 | tf_op jit(solution)/shard_map/all_to_all | solution.py:92
  266.1 2.5 all-reduce.1
  268.6 1.7 fusion.30
  (41 shorter events, 15.5 us)
Async XLA Ops:
  6.5 9.5 %copy-start.5 = (bf16[512,256]{1,0:T(8,128)(2,1)S(1)}, bf16[512,256]{1,0:T(8,128)(2,1)}, u32[]{:S(2)}) copy-start(bf16[512,256]{1,0:T(8,128)(2,1)} %param.16) | copy-start | bytes 786436
  6.5 47.8 %all-gather.11.cloned.1.call-start = ((), (), s32[]{:S(2)}) async-start(), calls=%async_computation.7 | async-start | bytes 2228224 | tf_op jit(solution)/shard_map/all_gather | solution.py:45
  10.3 20.9 %all-to-all-start = ((bf16[256,8,128]{0,2,1:T(8,128)(2,1)}), bf16[256,8,128]{0,2,1:T(8,128)(2,1)S(1)}, u32[]{:S(2)}, u32[]{:S(2)}) async-start(bf16[256,8,128]{0,2,1:T(8,128)(2,1)} %pad_maximum_fusion.1), calls=%async_computation | async-start | bytes 1048576 | tf_op jit(solution)/shard_map/all_to_all | solution.py:51
  31.2 27.5 %all-to-all-start.1 = ((bf16[512,2,128]{0,2,1:T(8,128)(2,1)}), bf16[512,2,128]{0,2,1:T(8,128)(2,1)S(1)}, u32[]{:S(2)}, u32[]{:S(2)}) async-start(bf16[512,2,128]{0,2,1:T(8,128)(2,1)} %bitcast.40), calls=%async_computation.1 | async-start | bytes 524288 | tf_op jit(solution)/shard_map/all_to_all | solution.py:54
  58.7 0.7 copy-start.4
  59.5 38.5 %all-to-all-start.3 = ((bf16[8,352,256]{2,1,0:T(8,128)(2,1)}), bf16[8,352,256]{2,1,0:T(8,128)(2,1)S(1)}, u32[]{:S(2)}, u32[]{:S(2)}) async-start(bf16[8,352,256]{2,1,0:T(8,128)(2,1)} %bitcast.121), calls=%async_computation.3 | async-start | bytes 2883584 | tf_op jit(solution)/shard_map/all_to_all | solution.py:58
  64.3 65.3 %all-gather.7.cloned.1.call-start = ((), (), s32[]{:S(2)}) async-start(), calls=%async_computation.5 | async-start | bytes 1114112 | tf_op jit(solution)/shard_map/all_gather | solution.py:72
  91.1 14.6 %copy-start.7 = (f32[512]{0:T(512)S(1)}, f32[512]{0:T(512)}, u32[]{:S(2)}) copy-start(f32[512]{0:T(512)} %param.15) | copy-start | bytes 6148
  98.0 76.6 %all-to-all-start.2 = ((bf16[256,8,704]{0,2,1:T(8,128)(2,1)}), bf16[256,8,704]{0,2,1:T(8,128)(2,1)}, u32[]{:S(2)}, u32[]{:S(2)}) async-start(bf16[256,8,704]{0,2,1:T(8,128)(2,1)} %pad_maximum_fusion), calls=%async_computation.2 | async-start | bytes 5767168 | tf_op jit(solution)/shard_map/all_to_all | solution.py:55
  103.9 95.9 %all-gather.9.cloned.1.call-start = ((), (), s32[]{:S(2)}) async-start(), calls=%async_computation.6 | async-start | bytes 2228224 | tf_op jit(solution)/shard_map/all_gather | solution.py:79
  178.4 24.2 %copy-start.6 = (f32[2048]{0:T(1024)S(1)}, f32[2048]{0:T(1024)}, u32[]{:S(2)}) copy-start(f32[2048]{0:T(1024)} %param.17) | copy-start | bytes 24580
  199.8 2.8 %copy-start = (bf16[512,2048]{1,0:T(8,128)(2,1)S(1)}, bf16[512,2048]{1,0:T(8,128)(2,1)}, u32[]{:S(2)}) copy-start(bf16[512,2048]{1,0:T(8,128)(2,1)} %all-gather.9.cloned.1.call-done) | copy-start | bytes 6291460
  202.6 1.8 copy-start.1
  203.6 2.4 copy-start.2
  204.4 1.7 copy-start.3
  214.1 50.5 %all-to-all-start.4 = ((bf16[16,64,1024]{2,1,0:T(8,128)(2,1)}), bf16[16,64,1024]{2,1,0:T(8,128)(2,1)S(1)}, u32[]{:S(2)}, u32[]{:S(2)}) async-start(bf16[16,64,1024]{2,1,0:T(8,128)(2,1)} %bitcast.112), calls=%async_computation.4 | async-start | bytes 4194304 | tf_op jit(solution)/shard_map/all_to_all | solution.py:92
  218.5 50.0 %dynamic-slice-start = ((f32[2048]{0:T(1024)}, s32[]{:T(128)}), f32[1024]{0:T(1024)S(1)}, s32[]{:S(2)}) async-start(f32[2048]{0:T(1024)} %param.21, s32[]{:T(128)} %select_n.9), calls=%async_computation.8 | async-start | bytes 8704 | tf_op jit(solution)/shard_map/dynamic_slice | solution.py:107
Sparse Core Ops, SparseCore 0:
  9.5 44.8 all-gather.10
  82.6 47.0 all-gather.6
  134.3 65.3 all-gather.8

commit v2 on v1

--- a/solution.py
+++ b/solution.py
@@ -1,6 +1,10 @@
+import functools
+
 import jax
 import jax.numpy as jnp
 from jax import lax
+from jax.experimental import pallas as pl
+from jax.experimental.pallas import tpu as pltpu
 from jax.sharding import PartitionSpec as P
 
 residual_scale = 2.0**0.25
@@ -22,12 +26,12 @@
     return pair.reshape(rows, 2 * width)
 
 
-def on_device(
+def by_collectives(
     tokens,
     lin_weight,
     glu_weight,
     conv_taps,
-    conv_gain_all,
+    conv_gain,
     conv_out_weight,
     mix_gain,
     ff_gate,
@@ -41,6 +45,7 @@
     groups = n_fs * seqs
     rows = groups * length
     model = feat * n_tp
+    conv_gain_all = lax.all_gather(conv_gain, "tp", axis=0, tiled=True)
 
     gathered = lax.all_gather(tokens, ("fs", "tp"), axis=0, tiled=False)
     all_tokens = (
@@ -108,6 +113,438 @@
     return (out * gain).astype(jnp.bfloat16).reshape(seqs, length, feat)
 
 
+MESH = pl.DeviceIdType.MESH
+LANES = 128
+
+
+def fused(
+    n_fs,
+    n_tp,
+    width,
+    tok,
+    glu_mix,
+    taps,
+    gain,
+    out_weight,
+    mix_gain,
+    gate_hbm,
+    up_hbm,
+    down_hbm,
+    out_gain,
+    out,
+    x_s,
+    glu_s,
+    gain_s,
+    proj_s,
+    pad_s,
+    conv_s,
+    norm_s,
+    act_s,
+    mixed_s,
+    mid_s,
+    gate_s,
+    up_s,
+    down_s,
+    hid_s,
+    part_s,
+    half_s,
+    sum_s,
+    q_s,
+    stat_s,
+    glu_sems,
+    small_sems,
+    tok_sems,
+    conv_sems,
+    mixed_sems,
+    ff_sems,
+    cross_sems,
+    local_sems,
+    half_sems,
+    q_sems,
+):
+    rep, f, t = lax.axis_index("rep"), lax.axis_index("fs"), lax.axis_index("tp")
+    other = 1 - t
+    n_hi = n_fs // 2
+    hi, lo = f // 2, f % 2
+    rows, feat = x_s.shape[1:]
+    length = rows // n_fs
+    model = feat * n_tp
+    depth = gate_hbm.shape[0]
+    half_depth = depth // 2
+    total = gate_hbm.shape[1]
+    chans = LANES // 2
+    pending = []
+
+    barrier = pltpu.get_barrier_semaphore()
+    for d in range(n_fs):
+        for e in range(n_tp):
+            if d or e:
+                pl.semaphore_signal(
+                    barrier,
+                    inc=1,
+                    device_id=(rep, (f + d) % n_fs, (t + e) % n_tp),
+                    device_id_type=MESH,
+                )
+    pl.semaphore_signal(barrier, inc=1, device_id=(1 - rep, f, t), device_id_type=MESH)
+    pl.semaphore_wait(barrier, n_fs * n_tp)
+
+    def remote(src, dst, sems, index, device):
+        return pltpu.make_async_remote_copy(
+            src_ref=src,
+            dst_ref=dst,
+            send_sem=sems.at[0, index],
+            recv_sem=sems.at[1, index],
+            device_id=device,
+            device_id_type=MESH,
+        )
+
+    def send(*parts):
+        copy = remote(*parts)
+        copy.start()
+        pending.append(copy)
+
+    partner = (rep, f, other)
+
+    def receive(dst, sems, index):
+        remote(dst, dst, sems, index, partner).wait_recv()
+
+    def at(step, low):
+        return ((hi - step + n_hi) % n_hi) * 2 + low
+
+    def gather_start(own, slot, sems):
+        for d in range(1, n_hi):
+            send(own, slot(f, t), sems, d, (rep, ((hi + d) % n_hi) * 2 + lo, t))
+        send(own, slot(f, t), sems, n_hi, (rep, hi * 2 + 1 - lo, t))
+        send(own, slot(f, t), sems, 2 * n_hi, partner)
+
+    def gather_finish(slot, sems):
+        for d in range(1, n_hi):
+            block = slot(at(d, lo), t)
+            receive(block, sems, d)
+            send(block, block, sems, n_hi + d, (rep, hi * 2 + 1 - lo, t))
+            send(block, block, sems, 2 * n_hi + d, partner)
+        for d in range(n_hi):
+            block = slot(at(d, 1 - lo), t)
+            receive(block, sems, n_hi + d)
+            send(block, block, sems, 3 * n_hi + d, partner)
+        for d in range(n_hi):
+            receive(slot(at(d, lo), other), sems, 2 * n_hi + d)
+            receive(slot(at(d, 1 - lo), other), sems, 3 * n_hi + d)
+
+    def tok_slot(i, j):
+        return x_s.at[j, pl.ds(pl.multiple_of(i * length, length), length)]
+
+    def glu_slot(i):
+        return glu_s.at[pl.ds(pl.multiple_of(i * depth, depth), depth)]
+
+    gather_start(tok, tok_slot, tok_sems)
+    for d in range(1, n_fs):
+        to = (f + d) % n_fs
+        send(glu_mix.at[to], glu_slot(f), glu_sems, d, (rep, to, t))
+    send(gain, gain_s.at[t], small_sems, 0, partner)
+    columns = pl.ds(pl.multiple_of(other * LANES, LANES), LANES)
+    own_columns = pl.ds(pl.multiple_of(t * LANES, LANES), LANES)
+    send(out_weight.at[:, columns], proj_s.at[t], small_sems, 1, partner)
+
+    def start_of(i):
+        return pl.multiple_of(i * width - (i // (n_fs - 1)) * (n_fs * width - total), LANES)
+
+    half_width = width // 2
+
+    def pieces(to, source, part):
+        first = start_of(to)
+        ups = pl.ds(pl.multiple_of(part * half_depth, half_depth), half_depth)
+        spot = pl.ds(pl.multiple_of(source * depth + part * half_depth, half_depth), half_depth)
+        deep = pl.ds(pl.multiple_of(part * half_width, half_width), half_width)
+        from_down = pl.ds(pl.multiple_of(first + part * half_width, LANES // 2), half_width)
+        return (
+            (gate_hbm.at[ups, pl.ds(first, width)], gate_s.at[spot]),
+            (up_hbm.at[ups, pl.ds(first, width)], up_s.at[spot]),
+            (down_hbm.at[from_down], down_s.at[source, deep]),
+        )
+
+    order = range(1, n_fs)
+
+    def weights_start(which):
+        for d in order:
+            to = (f + d) % n_fs
+            src, dst = pieces(to, f, rep)[which]
+            send(src, dst, ff_sems, which * n_fs + d, (rep, to, t))
+
+    def weights_forward(which):
+        for d in order:
+            dst = pieces(f, (f - d + n_fs) % n_fs, rep)[which][1]
+            receive(dst, ff_sems, which * n_fs + d)
+            send(dst, dst, cross_sems, which * n_fs + d, (1 - rep, f, t))
+
+    def weights_finish(which):
+        for d in order:
+            dst = pieces(f, (f - d + n_fs) % n_fs, 1 - rep)[which][1]
+            receive(dst, cross_sems, which * n_fs + d)
+
+    weights_start(0)
+    weights_start(1)
+    own_copies = []
+    for which in range(3):
+        for part in range(2):
+            src, dst = pieces(f, f, part)[which]
+            own_copies.append(
+                pltpu.make_async_copy(src, dst, local_sems.at[which * 2 + part])
+            )
+    for copy in own_copies:
+        copy.start()
+
+    x_s[t, pl.ds(pl.multiple_of(f * length, length), length), :] = tok[...]
+    glu_s[pl.ds(pl.multiple_of(f * depth, depth), depth), :] = glu_mix[f]
+    gain_s[t] = gain[...]
+    proj_s[t] = out_weight[:, own_columns]
+    pad_s[...] = jnp.zeros_like(pad_s)
+
+    gather_finish(tok_slot, tok_sems)
+    for d in range(1, n_fs):
+        receive(glu_slot((f - d + n_fs) % n_fs), glu_sems, d)
+
+    product = sum(
+        jnp.dot(
+            x_s[j], glu_s[j * feat : (j + 1) * feat], preferred_element_type=jnp.float32
+        )
+        for j in range(n_tp)
+    )
+    glu = product[:, :chans] / (1.0 + jnp.exp(-product[:, chans:]))
+    top = rows // 2
+    packed = jnp.concatenate((glu[:top], glu[top:]), axis=1)
+    packed = packed.astype(jnp.bfloat16).astype(jnp.float32)
+    n_taps = taps.shape[0]
+    margin = (n_taps - 1) // 2
+    conv_slot = lambda i, j: conv_s.at[j * n_fs + i]
+    groups = n_fs // 2
+    for g in range(groups):
+        pad_s[g, 16 : 16 + length, :] = packed[g * length : (g + 1) * length]
+    for g in range(groups):
+        acc = jnp.zeros((length, LANES), jnp.float32)
+        for k in range(n_taps):
+            first = 16 - margin + k
+            acc = acc + pad_s[g, first : first + length, :] * taps[k : k + 1, :]
+        conv_s[t * n_fs + f, g * length : (g + 1) * length, :] = acc.astype(jnp.bfloat16)
+    gather_start(conv_slot(f, t), conv_slot, conv_sems)
+    weights_forward(0)
+    gather_finish(conv_slot, conv_sems)
+    receive(gain_s.at[other], small_sems, 0)
+    receive(proj_s.at[other], small_sems, 1)
+
+    for j in range(n_fs * n_tp // 2):
+        left = conv_s[2 * j].astype(jnp.float32)
+        right = conv_s[2 * j + 1].astype(jnp.float32)
+        cols = slice(j * LANES, (j + 1) * LANES)
+        norm_s[:top, cols] = jnp.concatenate((left[:, :chans], right[:, :chans]), axis=1)
+        norm_s[top:, cols] = jnp.concatenate((left[:, chans:], right[:, chans:]), axis=1)
+    gains = jnp.concatenate([gain_s[j] for j in range(n_tp)], axis=1)
+
+    @pl.loop(0, n_fs)
+    def _(i):
+        here = pl.ds(pl.multiple_of(i * length, length), length)
+        v = normed(norm_s[here, :]) * gains
+        act_s[here, :] = (v / (1.0 + jnp.exp(-v))).astype(jnp.bfloat16)
+
+    share = proj_s.shape[1]
+    mixed_slot = lambda i, j: mixed_s.at[i * n_tp + j]
+    mixed_s[f * n_tp + t] = sum(
+        jnp.dot(
+            act_s[:, j * share : (j + 1) * share],
+            proj_s[j],
+            preferred_element_type=jnp.float32,
+        )
+        for j in range(n_tp)
+    ).astype(jnp.bfloat16)
+    gather_start(mixed_slot(f, t), mixed_slot, mixed_sems)
+    weights_start(2)
+    weights_forward(1)
+    gather_finish(mixed_slot, mixed_sems)
+
+    @pl.loop(0, n_fs)
+    def _(i):
+        here = pl.ds(pl.multiple_of(i * length, length), length)
+        skip = jnp.concatenate([x_s[j, here, :] for j in range(n_tp)], axis=1)
+        added = jnp.concatenate([mixed_s[j, here, :] for j in range(n_fs * n_tp)], axis=1)
+        before = residual_scale * skip.astype(jnp.float32) + added.astype(jnp.float32)
+        mid_s[here, :] = (normed(before) * mix_gain[...]).astype(jnp.bfloat16)
+
+    for copy in own_copies:
+        copy.wait()
+    weights_finish(0)
+    weights_finish(1)
+    weights_forward(2)
+    keep = lax.broadcasted_iota(jnp.int32, (1, width), 1) + start_of(f) >= f * width
+
+    @pl.loop(0, 2)
+    def _(i):
+        here = pl.ds(pl.multiple_of(i * top, top), top)
+        gate = jnp.dot(mid_s[here, :], gate_s[...], preferred_element_type=jnp.float32)
+        upward = jnp.dot(mid_s[here, :], up_s[...], preferred_element_type=jnp.float32)
+        value = gate / (1.0 + jnp.exp(-gate)) * upward
+        hid_s[here, :] = jnp.where(keep, value, 0.0).astype(jnp.bfloat16)
+
+    weights_finish(2)
+    span = down_s.shape[2]
+    per_half = n_fs // n_tp
+
+    @pl.loop(0, n_fs)
+    def _(j):
+        place = pl.ds(pl.multiple_of((j % per_half) * span, span), span)
+        part_s[j // per_half, :, place] = jnp.dot(
+            hid_s[...], down_s[j], preferred_element_type=jnp.float32
+        ).astype(jnp.bfloat16)
+
+    def rows_of(i):
+        return pl.ds(pl.multiple_of(i * length, length), length)
+
+    for d in list(range(1, n_fs)) + [0]:
+        here = rows_of((f + d) % n_fs)
+        send(part_s.at[other, here], half_s.at[here], half_sems, d, partner)
+    for d in list(range(1, n_fs)) + [0]:
+        to = (f + d) % n_fs
+        here = rows_of(to)
+        receive(half_s.at[here], half_sems, d)
+        both = part_s[t, here, :].astype(jnp.float32) + half_s[here, :].astype(jnp.float32)
+        sum_s[here, :] = both.astype(jnp.bfloat16)
+        if d:
+            send(sum_s.at[here], q_s.at[f], q_sems, d, (rep, to, t))
+    forward = sum_s[rows_of(f), :].astype(jnp.float32)
+    for d in range(1, n_fs):
+        source = (f - d + n_fs) % n_fs
+        receive(q_s.at[source], q_sems, d)
+        forward = forward + q_s[source].astype(jnp.float32)
+    forward = forward.astype(jnp.bfloat16).astype(jnp.float32)
+    own_half = pl.ds(pl.multiple_of(t * feat, feat), feat)
+    final = residual_scale * mid_s[rows_of(f), own_half].astype(jnp.float32) + forward
+    lane = lax.broadcasted_iota(jnp.int32, (length, LANES), 1)
+    stat_s[t] = jnp.where(
+        lane == 0,
+        jnp.sum(final, axis=1, keepdims=True),
+        jnp.sum(final * final, axis=1, keepdims=True),
+    )
+    send(stat_s.at[t], stat_s.at[t], small_sems, 2, partner)
+    receive(stat_s.at[other], small_sems, 2)
+    stats = (stat_s[0] + stat_s[1]) / model
+    average, second = stats[:, 0:1], stats[:, 1:2]
+    scaled = (final - average) * lax.rsqrt(second - average * average + epsilon)
+    out[...] = (scaled * out_gain[t]).astype(jnp.bfloat16)
+    for copy in pending:
+        copy.wait_send()
+
+
+def by_kernel(
+    width,
+    tokens,
+    lin_weight,
+    glu_weight,
+    conv_taps,
+    conv_gain,
+    conv_out_weight,
+    mix_gain,
+    ff_gate,
+    ff_up,
+    ff_down,
+    out_gain,
+):
+    n_fs, n_tp = lax.axis_size("fs"), lax.axis_size("tp")
+    _, length, feat = tokens.shape
+    rows, model = n_fs * length, feat * n_tp
+    depth, own_chans = lin_weight.shape
+    chans = own_chans // n_fs
+    n_taps = conv_taps.shape[0]
+    glu_mix = jnp.concatenate(
+        (
+            lin_weight.reshape(depth, n_fs, chans).transpose(1, 0, 2),
+            glu_weight.reshape(depth, n_fs, chans).transpose(1, 0, 2),
+        ),
+        axis=2,
+    )
+    own_taps = lax.dynamic_slice_in_dim(conv_taps, lax.axis_index("fs") * chans, chans, 1)
+    taps = jnp.concatenate((own_taps, own_taps), axis=1)
+    vmem, far = pl.BlockSpec(memory_space=pltpu.VMEM), pl.BlockSpec(memory_space=pl.ANY)
+    bf, fl = jnp.bfloat16, jnp.float32
+    span = ff_down.shape[1]
+    pair = lambda n: pltpu.SemaphoreType.DMA((2, n))
+    result = pl.pallas_call(
+        functools.partial(fused, n_fs, n_tp, width),
+        out_shape=jax.ShapeDtypeStruct((length, feat), bf),
+        in_specs=[vmem] * 6 + [far] * 3 + [vmem],
+        out_specs=vmem,
+        scratch_shapes=[
+            pltpu.VMEM((n_tp, rows, feat), bf),
+            pltpu.VMEM((n_fs * depth, 2 * chans), bf),
+            pltpu.VMEM((n_tp, 1, own_chans), fl),
+            pltpu.VMEM((n_tp, own_chans, span // n_tp), bf),
+            pltpu.VMEM((n_fs // 2, length + 32, LANES), fl),
+            pltpu.VMEM((n_fs * n_tp, rows // 2, LANES), bf),
+            pltpu.VMEM((rows, own_chans * n_tp), fl),
+            pltpu.VMEM((rows, own_chans * n_tp), bf),
+            pltpu.VMEM((n_fs * n_tp, rows, LANES), bf),
+            pltpu.VMEM((rows, model), bf),
+            pltpu.VMEM((n_fs * depth, width), bf),
+            pltpu.VMEM((n_fs * depth, width), bf),
+            pltpu.VMEM((n_fs, width, span), bf),
+            pltpu.VMEM((rows, width), bf),
+            pltpu.VMEM((n_tp, rows, feat), bf),
+            pltpu.VMEM((rows, feat), bf),
+            pltpu.VMEM((rows, feat), bf),
+            pltpu.VMEM((n_fs, length, feat), bf),
+            pltpu.VMEM((n_tp, length, LANES), fl),
+            pair(n_fs),
+            pair(3),
+            pair(2 * n_fs),
+            pair(2 * n_fs),
+            pair(2 * n_fs),
+            pair(3 * n_fs),
+            pair(3 * n_fs),
+            pltpu.SemaphoreType.DMA((6,)),
+            pair(n_fs),
+            pair(n_fs),
+        ],
+        compiler_params=pltpu.CompilerParams(
+            collective_id=0, has_side_effects=True, vmem_limit_bytes=60 * 2**20
+        ),
+    )(
+        tokens[0],
+        glu_mix,
+        taps,
+        conv_gain[None],
+        conv_out_weight,
+        mix_gain[None],
+        ff_gate,
+        ff_up,
+        ff_down,
+        out_gain.reshape(n_tp, 1, feat),
+    )
+    return result[None]
+
+
+def on_device(*args):
+    tokens, lin_weight, conv_out_weight, ff_gate = args[0], args[1], args[5], args[7]
+    n_fs, n_tp, n_rep = (lax.axis_size(a) for a in ("fs", "tp", "rep"))
+    seqs, length, feat = tokens.shape
+    units = ff_gate.shape[1]
+    width = -(-units // (n_fs * LANES)) * LANES
+    fits = (
+        n_rep == 2
+        and n_tp == 2
+        and n_fs % 4 == 0
+        and seqs == 1
+        and length % 16 == 0
+        and args[3].shape[0] <= 33
+        and lin_weight.shape[1] * 2 == n_fs * LANES
+        and conv_out_weight.shape[1] == n_tp * LANES
+        and feat % LANES == 0
+        and units % LANES == 0
+        and width * (n_fs - 1) < units
+        and lin_weight.shape[0] % 32 == 0
+    )
+    if fits:
+        return by_kernel(width, *args)
+    return by_collectives(*args)
+
+
 def solution(mesh):
     mapped = jax.shard_map(
         on_device,
@@ -117,7 +554,7 @@
             P("fs", "tp"),
             P("fs", "tp"),
             P(None, "tp"),
-            P(),
+            P("tp"),
             P("tp", "fs"),
             P(),
             P("fs", "tp"),

time: 279 us -> 160 us (0.57)
  waiting for transfers between devices: 161 us -> 0 us
  Pallas kernels: 0 us -> 152 us
  local copies, waits for them, and re-layouts: 34 us -> 3.46 us
  starting transfers between devices: 27.8 us -> 0 us
  other arithmetic: 25.8 us -> 1.76 us
  between operations: 13.3 us -> 0.04 us
  matrix products: 9.17 us -> 0 us
  blocking collectives: 5.76 us -> 0 us
    pallas_call x0 -> x1, Pallas kernels: none -> 152 us  [by_kernel(): pl.pallas_call(functools.partial(fused, n_fs, n_tp, width), out_shape=jax...]
    all_to_all x5 -> x0, waiting for transfers between devices: 103 us -> none  [the longest x1 46.1 us: on_device(): lax.all_to_all(sends, ('fs', 'tp'), split_axis=0, concat_axis=0, tiled=True)]
    all_gather x3 -> x0, waiting for transfers between devices: 57.3 us -> none  [the longest x1 21.4 us: on_device(): mixed = lax.all_gather(mixed_own, ('fs', 'tp'), axis=1, tiled=True)]
    all_to_all x5 -> x0, starting transfers between devices: 27.8 us -> none  [the longest x1 6.9 us: on_device(): lax.all_to_all(conv_out_weight, 'tp', split_axis=1, concat_axis=0, tiled=...]
    convert_element_type x2 -> x0, other arithmetic: 13.1 us -> none  [the longest x1 12.1 us: on_device(): conv = conv.reshape(rows, chans).astype(jnp.bfloat16)]
    reshape x4 -> x2, local copies, waits for them, and re-layouts: 10.7 us -> 0.55 us  [the longest x1 0.28 us: by_kernel(): glu_weight.reshape(depth, n_fs, chans).transpose(1, 0, 2)]
    dot_general x4 -> x0, matrix products: 9.17 us -> none  [the longest x1 2.93 us: on_device(): jnp.dot(activated, own_out, preferred_element_type=jnp.float32)]
    all_to_all x4 -> x0, local copies, waits for them, and re-layouts: 7.99 us -> none  [the longest x1 3.8 us: on_device(): lax.all_to_all(interleave(ff_gate, ff_up, n_fs), 'fs', split_axis=1, conc...]
  transfers between devices with their start and end apart: 8 -> 0, of which waited for: 7 -> 0; matrix products, arithmetic and copies ran while one was open for 18% -> 0% of each run, Pallas kernels for 0% -> 0%
where the time goes in v2:
time: 160 us; the launch traced here: 157 us
  Pallas kernels  152 us (95%)
  local copies, waits for them, and re-layouts  3.46 us (2%)
  other arithmetic  1.76 us (1%)
    pallas_call x1, Pallas kernels, by_kernel(): pl.pallas_call(functools.partial(fused, n_fs, n_tp, width), out_shape=jax...  152 us

profile of v2, /device:TPU:11, one launch (start us, length us, event | category | flops | bytes accessed | tf_op | source)
XLA Modules:
  0.0 157.0 jit_solution(10545207087003018079)
XLA Ops:
  0.0 0.0 copy-start
  0.0 0.0 copy-start.1
  0.0 1.1 copy.14
  1.1 0.3 copy.15
  1.4 0.0 copy-done.1
  1.4 0.1 copy.12
  1.6 0.3 copy.13
  1.9 1.1 pad_maximum_fusion.glu_mix
  2.9 0.0 copy-done
  2.9 0.1 constant_dynamic-slice_fusion
  3.0 0.7 pad_maximum_fusion.1.taps
  3.7 151.7 %shard_map.109 = bf16[64,1024]{1,0:T(8,128)(2,1)} custom-call(bf16[64,1024]{1,0:T(8,128)(2,1)} %bitcast.14, bf16[8,256,128]{2,1,0:T(8,128)(2,1)} %pad_maximum_fusion.glu_mix, f32[31,128]{1,0:T(8,128)} %pad_maximum_fusion.1.taps, f32[1,512]{1,0:T(1,128)} %bitcast.17, bf16[512,256]{1,0:T(8,128)(2,1)} %out_weight.1, f32[1,2048]{1,0:T(1,128)} %bitcast.15, ...), custom_call_target="tpu_custom_call" | custom-call | tf_op jit(solution)/shard_map/pallas_call | solution.py:469
  155.4 1.6 copy.17
Async XLA Ops:
  0.0 2.9 %copy-start = (f32[31,512]{1,0:T(8,128)S(1)}, f32[31,512]{1,0:T(8,128)}, u32[]{:S(2)}) copy-start(f32[31,512]{1,0:T(8,128)} %param.14) | copy-start | bytes 190468
  0.0 1.4 copy-start.1

commit v3 on v2

--- a/solution.py
+++ b/solution.py
@@ -161,6 +161,9 @@
     local_sems,
     half_sems,
     q_sems,
+    y_s,
+    y_sems,
+    glu_cross_sems,
 ):
     rep, f, t = lax.axis_index("rep"), lax.axis_index("fs"), lax.axis_index("tp")
     other = 1 - t
@@ -234,13 +237,19 @@
     def tok_slot(i, j):
         return x_s.at[j, pl.ds(pl.multiple_of(i * length, length), length)]
 
-    def glu_slot(i):
-        return glu_s.at[pl.ds(pl.multiple_of(i * depth, depth), depth)]
+    def half_rows(i, part):
+        return pl.ds(pl.multiple_of(i * depth + part * half_depth, half_depth), half_depth)
 
     gather_start(tok, tok_slot, tok_sems)
     for d in range(1, n_fs):
         to = (f + d) % n_fs
-        send(glu_mix.at[to], glu_slot(f), glu_sems, d, (rep, to, t))
+        send(
+            glu_mix.at[to, half_rows(0, rep)],
+            glu_s.at[half_rows(f, rep)],
+            glu_sems,
+            d,
+            (rep, to, t),
+        )
     send(gain, gain_s.at[t], small_sems, 0, partner)
     columns = pl.ds(pl.multiple_of(other * LANES, LANES), LANES)
     own_columns = pl.ds(pl.multiple_of(t * LANES, LANES), LANES)
@@ -264,14 +273,15 @@
         )
 
     order = range(1, n_fs)
-
-    def weights_start(which):
+    early, late = range(1, n_fs // 2 + 1), range(n_fs // 2 + 1, n_fs)
+
+    def weights_start(which, order=order):
         for d in order:
             to = (f + d) % n_fs
             src, dst = pieces(to, f, rep)[which]
             send(src, dst, ff_sems, which * n_fs + d, (rep, to, t))
 
-    def weights_forward(which):
+    def weights_forward(which, order=order):
         for d in order:
             dst = pieces(f, (f - d + n_fs) % n_fs, rep)[which][1]
             receive(dst, ff_sems, which * n_fs + d)
@@ -302,7 +312,12 @@
 
     gather_finish(tok_slot, tok_sems)
     for d in range(1, n_fs):
-        receive(glu_slot((f - d + n_fs) % n_fs), glu_sems, d)
+        block = glu_s.at[half_rows((f - d + n_fs) % n_fs, rep)]
+        receive(block, glu_sems, d)
+        send(block, block, glu_cross_sems, d, (1 - rep, f, t))
+    for d in range(1, n_fs):
+        block = glu_s.at[half_rows((f - d + n_fs) % n_fs, 1 - rep)]
+        receive(block, glu_cross_sems, d)
 
     product = sum(
         jnp.dot(
@@ -327,7 +342,9 @@
             acc = acc + pad_s[g, first : first + length, :] * taps[k : k + 1, :]
         conv_s[t * n_fs + f, g * length : (g + 1) * length, :] = acc.astype(jnp.bfloat16)
     gather_start(conv_slot(f, t), conv_slot, conv_sems)
+    weights_start(2, early)
     weights_forward(0)
+    weights_forward(1)
     gather_finish(conv_slot, conv_sems)
     receive(gain_s.at[other], small_sems, 0)
     receive(proj_s.at[other], small_sems, 1)
@@ -357,8 +374,8 @@
         for j in range(n_tp)
     ).astype(jnp.bfloat16)
     gather_start(mixed_slot(f, t), mixed_slot, mixed_sems)
-    weights_start(2)
-    weights_forward(1)
+    weights_start(2, late)
+    weights_forward(2, early)
     gather_finish(mixed_slot, mixed_sems)
 
     @pl.loop(0, n_fs)
@@ -373,47 +390,60 @@
         copy.wait()
     weights_finish(0)
     weights_finish(1)
-    weights_forward(2)
     keep = lax.broadcasted_iota(jnp.int32, (1, width), 1) + start_of(f) >= f * width
 
-    @pl.loop(0, 2)
-    def _(i):
-        here = pl.ds(pl.multiple_of(i * top, top), top)
+    for i in range(2):
+        here = pl.ds(i * top, top)
         gate = jnp.dot(mid_s[here, :], gate_s[...], preferred_element_type=jnp.float32)
         upward = jnp.dot(mid_s[here, :], up_s[...], preferred_element_type=jnp.float32)
         value = gate / (1.0 + jnp.exp(-gate)) * upward
         hid_s[here, :] = jnp.where(keep, value, 0.0).astype(jnp.bfloat16)
+        if i == 0:
+            weights_forward(2, late)
 
     weights_finish(2)
     span = down_s.shape[2]
     per_half = n_fs // n_tp
 
-    @pl.loop(0, n_fs)
-    def _(j):
-        place = pl.ds(pl.multiple_of((j % per_half) * span, span), span)
-        part_s[j // per_half, :, place] = jnp.dot(
-            hid_s[...], down_s[j], preferred_element_type=jnp.float32
-        ).astype(jnp.bfloat16)
+    def project(side):
+        @pl.loop(0, per_half)
+        def _(j):
+            part_s[side, :, pl.ds(pl.multiple_of(j * span, span), span)] = jnp.dot(
+                hid_s[...], down_s[side * per_half + j], preferred_element_type=jnp.float32
+            ).astype(jnp.bfloat16)
 
     def rows_of(i):
         return pl.ds(pl.multiple_of(i * length, length), length)
 
-    for d in list(range(1, n_fs)) + [0]:
-        here = rows_of((f + d) % n_fs)
-        send(part_s.at[other, here], half_s.at[here], half_sems, d, partner)
-    for d in list(range(1, n_fs)) + [0]:
-        to = (f + d) % n_fs
-        here = rows_of(to)
-        receive(half_s.at[here], half_sems, d)
+    def toward(step, low):
+        return ((hi + step) % n_hi) * 2 + low
+
+    steps = list(range(1, n_hi)) + [0]
+    project(other)
+    for d in steps:
+        for e, low in enumerate((1 - lo, lo)):
+            here = rows_of(toward(d, low))
+            send(part_s.at[other, here], half_s.at[here], half_sems, 2 * d + e, partner)
+    project(t)
+    for d in steps:
+        here = rows_of(toward(d, 1 - lo))
+        receive(half_s.at[here], half_sems, 2 * d)
         both = part_s[t, here, :].astype(jnp.float32) + half_s[here, :].astype(jnp.float32)
         sum_s[here, :] = both.astype(jnp.bfloat16)
+        send(sum_s.at[here], y_s.at[d], y_sems, d, (rep, hi * 2 + 1 - lo, t))
+    for d in steps:
+        to = toward(d, lo)
+        here = rows_of(to)
+        receive(half_s.at[here], half_sems, 2 * d + 1)
+        both = part_s[t, here, :].astype(jnp.float32) + half_s[here, :].astype(jnp.float32)
+        receive(y_s.at[d], y_sems, d)
+        forward = both + y_s[d].astype(jnp.float32)
         if d:
-            send(sum_s.at[here], q_s.at[f], q_sems, d, (rep, to, t))
-    forward = sum_s[rows_of(f), :].astype(jnp.float32)
-    for d in range(1, n_fs):
-        source = (f - d + n_fs) % n_fs
-        receive(q_s.at[source], q_sems, d)
-        forward = forward + q_s[source].astype(jnp.float32)
+            sum_s[here, :] = forward.astype(jnp.bfloat16)
+            send(sum_s.at[here], q_s.at[d], q_sems, d, (rep, to, t))
+    for d in range(1, n_hi):
+        receive(q_s.at[d], q_sems, d)
+        forward = forward + q_s[d].astype(jnp.float32)
     forward = forward.astype(jnp.bfloat16).astype(jnp.float32)
     own_half = pl.ds(pl.multiple_of(t * feat, feat), feat)
     final = residual_scale * mid_s[rows_of(f), own_half].astype(jnp.float32) + forward
@@ -489,7 +519,7 @@
             pltpu.VMEM((n_tp, rows, feat), bf),
             pltpu.VMEM((rows, feat), bf),
             pltpu.VMEM((rows, feat), bf),
-            pltpu.VMEM((n_fs, length, feat), bf),
+            pltpu.VMEM((n_fs // 2, length, feat), bf),
             pltpu.VMEM((n_tp, length, LANES), fl),
             pair(n_fs),
             pair(3),
@@ -500,6 +530,9 @@
             pair(3 * n_fs),
             pltpu.SemaphoreType.DMA((6,)),
             pair(n_fs),
+            pair(n_fs // 2),
+            pltpu.VMEM((n_fs // 2, length, feat), bf),
+            pair(n_fs // 2),
             pair(n_fs),
         ],
         compiler_params=pltpu.CompilerParams(

time: 160 us -> 145 us (0.906); the launches traced: 157 us -> 145 us
  Pallas kernels: 152 us -> 139 us
    pallas_call x1, Pallas kernels: 152 us -> 139 us  [by_kernel(): pl.pallas_call(functools.partial(fused, n_fs, n_tp, width), out_shape=jax...]
where the time goes in v3:
time: 145 us
  Pallas kernels  139 us (96%)
  local copies, waits for them, and re-layouts  3.46 us (2%)
  other arithmetic  1.76 us (1%)
    pallas_call x1, Pallas kernels, by_kernel(): pl.pallas_call(functools.partial(fused, n_fs, n_tp, width), out_shape=jax...  139 us

profile of v3, /device:TPU:11, one launch (start us, length us, event | category | flops | bytes accessed | tf_op | source)
XLA Modules:
  0.0 144.7 jit_solution(14268505137644296270)
XLA Ops:
  0.0 0.0 copy-start
  0.0 0.0 copy-start.1
  0.0 1.1 copy.14
  1.1 0.3 copy.15
  1.4 0.0 copy-done.1
  1.4 0.1 copy.12
  1.6 0.3 copy.13
  1.9 1.1 pad_maximum_fusion.glu_mix
  2.9 0.0 copy-done
  2.9 0.1 constant_dynamic-slice_fusion
  3.0 0.7 pad_maximum_fusion.1.taps
  3.7 139.4 %shard_map.109 = bf16[64,1024]{1,0:T(8,128)(2,1)} custom-call(bf16[64,1024]{1,0:T(8,128)(2,1)} %bitcast.14, bf16[8,256,128]{2,1,0:T(8,128)(2,1)} %pad_maximum_fusion.glu_mix, f32[31,128]{1,0:T(8,128)} %pad_maximum_fusion.1.taps, f32[1,512]{1,0:T(1,128)} %bitcast.17, bf16[512,256]{1,0:T(8,128)(2,1)} %out_weight.1, f32[1,2048]{1,0:T(1,128)} %bitcast.15, ...), custom_call_target="tpu_custom_call" | custom-call | tf_op jit(solution)/shard_map/pallas_call | solution.py:499
  143.1 1.6 %copy.17 = bf16[1,64,1024]{2,1,0:T(8,128)(2,1)} copy(bf16[1,64,1024]{2,1,0:T(8,128)(2,1)} %bitcast.13) | data formatting | bytes 262144
Async XLA Ops:
  0.0 2.9 %copy-start = (f32[31,512]{1,0:T(8,128)S(1)}, f32[31,512]{1,0:T(8,128)}, u32[]{:S(2)}) copy-start(f32[31,512]{1,0:T(8,128)} %param.14) | copy-start | bytes 190468
  0.0 1.4 copy-start.1

commit v4 on v3

--- a/solution.py
+++ b/solution.py
@@ -273,7 +273,8 @@
         )
 
     order = range(1, n_fs)
-    early, late = range(1, n_fs // 2 + 1), range(n_fs // 2 + 1, n_fs)
+    early, late = range(1, n_fs // 4 + 1), range(n_fs // 4 + 1, n_fs)
+    near, rest = range(1, n_fs // 2 + 1), range(n_fs // 2 + 1, n_fs)
 
     def weights_start(which, order=order):
         for d in order:
@@ -293,7 +294,6 @@
             receive(dst, cross_sems, which * n_fs + d)
 
     weights_start(0)
-    weights_start(1)
     own_copies = []
     for which in range(3):
         for part in range(2):
@@ -342,9 +342,9 @@
             acc = acc + pad_s[g, first : first + length, :] * taps[k : k + 1, :]
         conv_s[t * n_fs + f, g * length : (g + 1) * length, :] = acc.astype(jnp.bfloat16)
     gather_start(conv_slot(f, t), conv_slot, conv_sems)
+    weights_start(1)
     weights_start(2, early)
     weights_forward(0)
-    weights_forward(1)
     gather_finish(conv_slot, conv_sems)
     receive(gain_s.at[other], small_sems, 0)
     receive(proj_s.at[other], small_sems, 1)
@@ -363,6 +363,7 @@
         v = normed(norm_s[here, :]) * gains
         act_s[here, :] = (v / (1.0 + jnp.exp(-v))).astype(jnp.bfloat16)
 
+    weights_forward(1, near)
     share = proj_s.shape[1]
     mixed_slot = lambda i, j: mixed_s.at[i * n_tp + j]
     mixed_s[f * n_tp + t] = sum(
@@ -375,6 +376,7 @@
     ).astype(jnp.bfloat16)
     gather_start(mixed_slot(f, t), mixed_slot, mixed_sems)
     weights_start(2, late)
+    weights_forward(1, rest)
     weights_forward(2, early)
     gather_finish(mixed_slot, mixed_sems)
 

time: 145 us -> 145 us (level)
  the two profiles are of different devices: /device:TPU:11 before, /device:TPU:13 now
where the time goes in v4:
time: 145 us
  Pallas kernels  140 us (97%)
  local copies, waits for them, and re-layouts  3.46 us (2%)
  other arithmetic  1.76 us (1%)
    pallas_call x1, Pallas kernels, by_kernel(): pl.pallas_call(functools.partial(fused, n_fs, n_tp, width), out_shape=jax...  140 us

profile of v4, /device:TPU:13, one launch (start us, length us, event | category | flops | bytes accessed | tf_op | source)
XLA Modules:
  0.0 145.3 jit_solution(15094547267410397341)
XLA Ops:
  0.0 0.0 copy-start
  0.0 0.0 copy-start.1
  0.0 1.1 copy.14
  1.1 0.3 copy.15
  1.4 0.0 copy-done.1
  1.4 0.1 copy.12
  1.6 0.3 copy.13
  1.9 1.1 pad_maximum_fusion.glu_mix
  2.9 0.0 copy-done
  2.9 0.1 constant_dynamic-slice_fusion
  3.0 0.7 pad_maximum_fusion.1.taps
  3.7 140.1 %shard_map.109 = bf16[64,1024]{1,0:T(8,128)(2,1)} custom-call(bf16[64,1024]{1,0:T(8,128)(2,1)} %bitcast.14, bf16[8,256,128]{2,1,0:T(8,128)(2,1)} %pad_maximum_fusion.glu_mix, f32[31,128]{1,0:T(8,128)} %pad_maximum_fusion.1.taps, f32[1,512]{1,0:T(1,128)} %bitcast.17, bf16[512,256]{1,0:T(8,128)(2,1)} %out_weight.1, f32[1,2048]{1,0:T(1,128)} %bitcast.15, ...), custom_call_target="tpu_custom_call" | custom-call | tf_op jit(solution)/shard_map/pallas_call | solution.py:501
  143.8 1.6 %copy.17 = bf16[1,64,1024]{2,1,0:T(8,128)(2,1)} copy(bf16[1,64,1024]{2,1,0:T(8,128)(2,1)} %bitcast.13) | data formatting | bytes 262144
Async XLA Ops:
  0.0 2.9 %copy-start = (f32[31,512]{1,0:T(8,128)S(1)}, f32[31,512]{1,0:T(8,128)}, u32[]{:S(2)}) copy-start(f32[31,512]{1,0:T(8,128)} %param.14) | copy-start | bytes 190468
  0.0 1.4 copy-start.1
